TPU v7x, 32 devices: a whole 2x2x4 slice. The times are simulated.
32 devices in a mesh: sp: 8 (over z, y), tp: 4 (over x, core).
Axes of the slice: x: 2, y: 2, z: 4, core: 2. Of those that a mesh axis runs over, the one named last changes fastest.
Arguments:
- tokens: bfloat16 [6144, 4096], P('sp', 'tp'), may hold values from -6 to 6
- in_proj: bfloat16 [3, 4096, 1024], P(None, 'tp', 'sp'), may hold values from -0.09375 to 0.09375
- group_mix: bfloat16 [3, 4, 256, 256], replicated, may hold values from -0.375 to 0.375
- pool_gain: float32 [3, 1024], replicated, may hold values from 0.1 to 1.9
- out_proj: bfloat16 [3, 1024, 4096], P(None, 'sp', 'tp'), may hold values from -0.1875 to 0.1875
- norm_gain: float32 [3, 4096], P(None, 'tp'), may hold values from 0.25 to 3
- norm_bias: float32 [3, 4096], P(None, 'tp'), may hold values from -1.5 to 1.5
Outputs:
- stream_out: bfloat16 [6144, 4096], P('sp', 'tp')
All inputs are finite; a program needn't handle non-finite values.
Results may differ from a plain program's by a relative error of at most 0.017.
Values may be sent and summed in bfloat16 or wider, within the bound.
A program may use at most 128 MiB of HBM per device.

v0:
```python
import jax
import jax.numpy as jnp
from jax import lax
from jax.sharding import PartitionSpec as P

pool_windows = (2, 4, 8, 16)
norm_eps = 1e-05


def padded(array, sides, width):
    for axis, dim in sides:
        devices, length = (lax.axis_size(axis), array.shape[dim])
        up = [(i, (i + 1) % devices) for i in range(devices - 1)]
        down = [(j, i) for i, j in up]
        last = lax.slice_in_dim(array, length - width, length, axis=dim)
        leading = lax.slice_in_dim(array, 0, width, axis=dim)
        before = lax.ppermute(last, axis, up)
        after = lax.ppermute(leading, axis, down)
        array = jnp.concatenate([before, array, after], axis=dim)
    return array


def on_device(tokens, in_proj, group_mix, pool_gain, out_proj, norm_gain, norm_bias):
    rows_dev = tokens.shape[0]
    feat_dev = tokens.shape[1]
    layer_count = in_proj.shape[0]
    pool_width = in_proj.shape[2] * lax.axis_size("sp")
    chan_share = pool_width // lax.axis_size("tp")
    group_width = group_mix.shape[2]
    model_width = feat_dev * lax.axis_size("tp")
    residual_scale = (2.0 * layer_count) ** 0.25
    fringe_width = max(pool_windows) // 2
    seq_length = rows_dev * lax.axis_size("sp")
    positions = lax.axis_index("sp") * rows_dev + jnp.arange(rows_dev)
    chan_groups = (lax.axis_index("tp") * chan_share + jnp.arange(chan_share)) // group_width
    in_all, out_all = (
        lax.all_gather(in_proj, "sp", axis=2, tiled=True),
        lax.all_gather(out_proj, "sp", axis=1, tiled=True),
    )
    stream = tokens
    for layer_idx in range(layer_count):
        in_block = in_all[layer_idx]
        out_block = out_all[layer_idx]
        projected = lax.psum_scatter(
            lax.dot_general(
                in_block, stream, (((0,), (1,)), ((), ())), preferred_element_type=jnp.float32
            ).astype(jnp.bfloat16),
            "tp",
            scatter_dimension=0,
            tiled=True,
        )
        extended = padded(projected, (("sp", 1),), fringe_width)
        ext_float = extended.astype(jnp.float32)
        pooled = jnp.zeros((chan_share, rows_dev), jnp.float32)
        for group_idx in range(4):
            own_rows = (chan_groups == group_idx)[:, None]
            span_len = pool_windows[group_idx]
            before = span_len // 2
            after = span_len - before
            window_total = jnp.zeros((ext_float.shape[0], rows_dev), jnp.float32)
            for offset in range(-before, after):
                window_total = (
                    window_total
                    + ext_float[:, fringe_width + offset : fringe_width + offset + rows_dev]
                )
            low_edge = jnp.clip(positions - before, 0, seq_length)
            high_edge = jnp.clip(positions + after, 0, seq_length)
            pooled = jnp.where(
                own_rows, window_total / (high_edge - low_edge).astype(jnp.float32)[None, :], pooled
            )
        differ = (pooled - projected.astype(jnp.float32)).astype(jnp.bfloat16)
        all_differ = lax.all_gather(differ, "tp", axis=0, tiled=True)
        grouped = all_differ.reshape(4, group_width, rows_dev)
        mixed_all = jnp.einsum(
            "gcd,gct->gdt", group_mix[layer_idx], grouped, preferred_element_type=jnp.float32
        ).reshape(pool_width, rows_dev)
        mixed_all = (mixed_all * pool_gain[layer_idx][:, None]).astype(jnp.bfloat16)
        branch = lax.dot_general(
            mixed_all, out_block, (((0,), (0,)), ((), ())), preferred_element_type=jnp.float32
        )
        resid = residual_scale * stream.astype(jnp.float32) + branch
        row_sums, squares = lax.psum((jnp.sum(resid, axis=1), jnp.sum(resid * resid, axis=1)), "tp")
        row_mean = row_sums / model_width
        row_var = squares / model_width - row_mean * row_mean
        normed = (resid - row_mean[:, None]) * lax.rsqrt(row_var[:, None] + norm_eps)
        stream = (normed * norm_gain[layer_idx][None, :] + norm_bias[layer_idx][None, :]).astype(
            jnp.bfloat16
        )
    return stream


def solution(mesh):
    in_specs = (
        P("sp", "tp"),
        P(None, "tp", "sp"),
        P(),
        P(),
        P(None, "sp", "tp"),
        P(None, "tp"),
        P(None, "tp"),
    )
    out_specs = P("sp", "tp")
    return jax.shard_map(
        on_device, mesh=mesh, in_specs=in_specs, out_specs=out_specs, check_vma=False
    )
```

profile of v0, /device:TPU:9, one launch (start us, length us, event | category | flops | bytes accessed | tf_op | source)
XLA Modules:
  0.0 466.5 jit_solution(7111326799867742258)
XLA Ops:
  7.3 100.2 %all-gather.6.cloned.1.call-done = bf16[3,1024,1024]{2,1,0:T(8,128)(2,1)} async-done(((bf16[3,1024,128]{2,1,0:T(8,128)(2,1)}), bf16[3,1024,1024]{2,1,0:T(8,128)(2,1)}) %all-gather.6.cloned.1.call-update) | async-done | bytes 6291472 | tf_op jit(solution)/shard_map/all_gather | solution.py:37
  107.5 5.0 %fusion.6 = bf16[1024,768]{1,0:T(8,128)(2,1)} fusion(bf16[768,1024]{1,0:T(8,128)(2,1)} %param.7, bf16[3,1024,1024]{2,1,0:T(8,128)(2,1)} %all-gather.6.cloned.1.call-done), kind=kOutput, calls=%fused_computation.24 | convolution fusion | flops 1611399168 | bytes 5242880 | tf_op jit(solution)/shard_map/dot_general | solution.py:45
  112.6 28.7 %reduce-scatter.4.cloned.1.call-done = bf16[256,768]{1,0:T(8,128)(2,1)} async-done(((bf16[1024,768]{1,0:T(8,128)(2,1)}), bf16[256,768]{1,0:T(8,128)(2,1)}) %reduce-scatter.4.cloned.1.call-update) | async-done | bytes 393232 | tf_op jit(solution)/shard_map/reduce_scatter | solution.py:44
  142.3 3.1 collective-permute-start
  151.7 5.1 %fusion.44 = bf16[256,768]{1,0:T(8,128)(2,1)} fusion(bf16[256,768]{1,0:T(8,128)(2,1)} %reduce-scatter.4.cloned.1.call-done, f32[256,784]{1,0:T(8,128)S(1)} %maximum_convert_fusion, f32[768]{0:T(1024)S(1)} %get-tuple-element.41, f32[768]{0:T(1024)S(1)} %get-tuple-element.42, f32[768]{0:T(1024)S(1)} %get-tuple-element.43, f32[768]{0:T(1024)S(1)} %get-tuple-element.44, ...), kind=kLoop, calls=%fused_computation.83 | loop fusion | flops 7274496 | bytes 13382656 | tf_op jit(solution)/shard_map/convert_element_type | solution.py:71
  157.5 21.0 %all-gather.8.cloned.1.call-done = bf16[1024,768]{1,0:T(8,128)(2,1)} async-done(((bf16[256,768]{1,0:T(8,128)(2,1)}), bf16[1024,768]{1,0:T(8,128)(2,1)}) %all-gather.8.cloned.1.call-update) | async-done | bytes 1572880 | tf_op jit(solution)/shard_map/all_gather | solution.py:72
  180.6 95.7 %all-gather.10.cloned.1.call-done = bf16[3,1024,1024]{2,1,0:T(8,128)(2,1)} async-done(((bf16[3,128,1024]{2,1,0:T(8,128)(2,1)}), bf16[3,1024,1024]{2,1,0:T(8,128)(2,1)}) %all-gather.10.cloned.1.call-update) | async-done | bytes 6291472 | tf_op jit(solution)/shard_map/all_gather | solution.py:38
  276.3 5.8 %fusion.55 = (f32[768]{0:T(1024)S(1)}, f32[768]{0:T(1024)S(1)}, f32[768,1024]{1,0:T(8,128)}) fusion(bf16[1024,768]{1,0:T(8,128)(2,1)S(1)} %bitcast.86, bf16[3,1024,1024]{2,1,0:T(8,128)(2,1)} %all-gather.10.cloned.1.call-done, bf16[768,1024]{1,0:T(8,128)(2,1)} %param.7), kind=kOutput, calls=%fused_computation.119 | convolution fusion | flops 1615329792 | bytes 8394752 | tf_op jit(solution)/shard_map/dot_general | solution.py:78
  282.1 7.2 %all-reduce.2 = (f32[768]{0:T(1024)S(1)}, f32[768]{0:T(1024)S(1)}) all-reduce(f32[768]{0:T(1024)S(1)} %get-tuple-element.10, f32[768]{0:T(1024)S(1)} %get-tuple-element.9), channel_id=1, replica_groups=mesh['sp'=8,'tp'=4] {'tp'}, use_global_device_ids=true, to_apply=%region_4.5 | all-reduce | flops 1536 | bytes 12288 | tf_op jit(solution)/shard_map/psum | solution.py:82
  289.3 5.9 %fusion.10 = bf16[1024,768]{1,0:T(8,128)(2,1)} fusion(bf16[3,1024,1024]{2,1,0:T(8,128)(2,1)} %all-gather.6.cloned.1.call-done, f32[768,1024]{1,0:T(8,128)} %get-tuple-element.38, f32[1024]{0:T(1024)S(1)} %bitcast.95, f32[1024]{0:T(1024)S(1)} %bitcast.93, f32[768]{0:T(1024)S(1)} %get-tuple-element.37, f32[768]{0:T(1024)S(1)} %get-tuple-element.36), kind=kOutput, calls=%fused_computation.28 | convolution fusion | flops 1615331328 | bytes 6830080 | tf_op jit(solution)/shard_map/dot_general | solution.py:45
  295.3 27.6 %reduce-scatter.6.cloned.1.call-done = bf16[256,768]{1,0:T(8,128)(2,1)} async-done(((bf16[1024,768]{1,0:T(8,128)(2,1)}), bf16[256,768]{1,0:T(8,128)(2,1)}) %reduce-scatter.6.cloned.1.call-update) | async-done | bytes 393232 | tf_op jit(solution)/shard_map/reduce_scatter | solution.py:44
  323.8 3.1 collective-permute-start.2
  333.2 5.0 %fusion.45 = bf16[256,768]{1,0:T(8,128)(2,1)} fusion(bf16[256,768]{1,0:T(8,128)(2,1)} %reduce-scatter.6.cloned.1.call-done, f32[256,784]{1,0:T(8,128)S(1)} %maximum_convert_fusion.1, f32[768]{0:T(1024)S(1)} %get-tuple-element.41, f32[768]{0:T(1024)S(1)} %get-tuple-element.42, f32[768]{0:T(1024)S(1)} %get-tuple-element.43, f32[768]{0:T(1024)S(1)} %get-tuple-element.44, ...), kind=kLoop, calls=%fused_computation.84 | loop fusion | flops 7274496 | bytes 13382656 | tf_op jit(solution)/shard_map/convert_element_type | solution.py:71
  338.4 21.5 %all-gather.12.cloned.1.call-done = bf16[1024,768]{1,0:T(8,128)(2,1)} async-done(((bf16[256,768]{1,0:T(8,128)(2,1)}), bf16[1024,768]{1,0:T(8,128)(2,1)}) %all-gather.12.cloned.1.call-update) | async-done | bytes 1572880 | tf_op jit(solution)/shard_map/all_gather | solution.py:72
  362.3 5.9 %fusion.54 = (f32[768]{0:T(1024)S(1)}, f32[768]{0:T(1024)S(1)}, f32[768,1024]{1,0:T(8,128)}) fusion(bf16[1024,768]{1,0:T(8,128)(2,1)S(1)} %bitcast.85, bf16[3,1024,1024]{2,1,0:T(8,128)(2,1)} %all-gather.10.cloned.1.call-done, f32[1024]{0:T(1024)S(1)} %bitcast.96, f32[1024]{0:T(1024)S(1)} %bitcast.94, f32[768]{0:T(1024)S(1)} %get-tuple-element.37, ...), kind=kOutput, calls=%fused_computation.118 | convolution fusion | flops 1619261952 | bytes 9981952 | tf_op jit(solution)/shard_map/dot_general | solution.py:78
  368.1 5.3 %all-reduce.1 = (f32[768]{0:T(1024)S(1)}, f32[768]{0:T(1024)S(1)}) all-reduce(f32[768]{0:T(1024)S(1)} %get-tuple-element.8, f32[768]{0:T(1024)S(1)} %get-tuple-element.7), channel_id=1, replica_groups=mesh['sp'=8,'tp'=4] {'tp'}, use_global_device_ids=true, to_apply=%region_9.10 | all-reduce | flops 1536 | bytes 12288 | tf_op jit(solution)/shard_map/psum | solution.py:82
  373.5 5.9 %fusion.9 = bf16[1024,768]{1,0:T(8,128)(2,1)} fusion(bf16[3,1024,1024]{2,1,0:T(8,128)(2,1)} %all-gather.6.cloned.1.call-done, f32[768,1024]{1,0:T(8,128)} %get-tuple-element.39, f32[1024]{0:T(1024)S(1)} %bitcast.91, f32[1024]{0:T(1024)S(1)} %bitcast.89, f32[768]{0:T(1024)S(1)} %get-tuple-element.35, f32[768]{0:T(1024)S(1)} %get-tuple-element.34), kind=kOutput, calls=%fused_computation.27 | convolution fusion | flops 1615331328 | bytes 6830080 | tf_op jit(solution)/shard_map/dot_general | solution.py:45
  379.5 29.3 %reduce-scatter.8.cloned.1.call-done = bf16[256,768]{1,0:T(8,128)(2,1)} async-done(((bf16[1024,768]{1,0:T(8,128)(2,1)}), bf16[256,768]{1,0:T(8,128)(2,1)}) %reduce-scatter.8.cloned.1.call-update) | async-done | bytes 393232 | tf_op jit(solution)/shard_map/reduce_scatter | solution.py:44
  409.7 3.1 collective-permute-start.4
  412.8 3.1 collective-permute-start.5
  419.1 5.0 %fusion.46 = bf16[256,768]{1,0:T(8,128)(2,1)} fusion(bf16[256,768]{1,0:T(8,128)(2,1)} %reduce-scatter.8.cloned.1.call-done, f32[256,784]{1,0:T(8,128)S(1)} %maximum_convert_fusion.2, f32[768]{0:T(1024)S(1)} %get-tuple-element.41, f32[768]{0:T(1024)S(1)} %get-tuple-element.42, f32[768]{0:T(1024)S(1)} %get-tuple-element.43, f32[768]{0:T(1024)S(1)} %get-tuple-element.44, ...), kind=kLoop, calls=%fused_computation.85 | loop fusion | flops 7274496 | bytes 13382656 | tf_op jit(solution)/shard_map/convert_element_type | solution.py:71
  424.0 21.8 %all-gather.14.cloned.1.call-done = bf16[1024,768]{1,0:T(8,128)(2,1)} async-done(((bf16[256,768]{1,0:T(8,128)(2,1)}), bf16[1024,768]{1,0:T(8,128)(2,1)}) %all-gather.14.cloned.1.call-update) | async-done | bytes 1572880 | tf_op jit(solution)/shard_map/all_gather | solution.py:72
  448.2 4.4 fusion.53
  452.5 5.4 %all-reduce = (f32[768]{0:T(1024)S(1)}, f32[768]{0:T(1024)S(1)}) all-reduce(f32[768]{0:T(1024)S(1)} %get-tuple-element.6, f32[768]{0:T(1024)S(1)} %get-tuple-element.5), channel_id=1, replica_groups=mesh['sp'=8,'tp'=4] {'tp'}, use_global_device_ids=true, to_apply=%region_14.15 | all-reduce | flops 1536 | bytes 12288 | tf_op jit(solution)/shard_map/psum | solution.py:82
  (59 shorter events, 28.8 us)
Async XLA Ops:
  6.5 100.9 %all-gather.6.cloned.1.call-start = ((), (), s32[]{:S(2)}) async-start(), calls=%async_computation.3 | async-start | bytes 7077888 | tf_op jit(solution)/shard_map/all_gather | solution.py:37
  7.3 134.1 %reduce-scatter.4.cloned.1.call-start = ((), (), s32[]{:S(2)}) async-start(), calls=%async_computation.4 | async-start | bytes 1966080 | tf_op jit(solution)/shard_map/reduce_scatter | solution.py:44
  112.5 66.0 %all-gather.8.cloned.1.call-start = ((), (), s32[]{:S(2)}) async-start(), calls=%async_computation.5 | async-start | bytes 1966080 | tf_op jit(solution)/shard_map/all_gather | solution.py:72
  142.3 6.2 %collective-permute-start = (bf16[256,8]{1,0:T(8,128)(2,1)S(1)}, bf16[256,8]{1,0:T(8,128)(2,1)S(1)}, u32[]{:S(2)}, u32[]{:S(2)}) collective-permute-start(bf16[256,8]{1,0:T(8,128)(2,1)S(1)} %get-tuple-element.24), channel_id=1, source_target_pairs={{0,4},{4,8},{8,12},{12,16},{16,20},{20,24},{24,28},{1,5},{5,9},{9,... | collective-permute-start | bytes 12296 | tf_op jit(solution)/shard_map/ppermute | solution.py:17
  145.4 5.0 %collective-permute-start.1 = (bf16[256,8]{1,0:T(8,128)(2,1)S(1)}, bf16[256,8]{1,0:T(8,128)(2,1)S(1)}, u32[]{:S(2)}, u32[]{:S(2)}) collective-permute-start(bf16[256,8]{1,0:T(8,128)(2,1)S(1)} %get-tuple-element.25), channel_id=1, source_target_pairs={{4,0},{8,4},{12,8},{16,12},{20,16},{24,20},{28,24},{5,1},{9,5},{13... | collective-permute-start | bytes 12296 | tf_op jit(solution)/shard_map/ppermute | solution.py:18
  151.6 5.8 %copy-start.1 = (f32[3,1024]{1,0:T(4,128)S(1)}, f32[3,1024]{1,0:T(4,128)}, u32[]{:S(2)}) copy-start(f32[3,1024]{1,0:T(4,128)} %param.10) | copy-start | bytes 36868
  151.6 5.8 %copy-start.2 = (f32[3,1024]{1,0:T(4,128)S(1)}, f32[3,1024]{1,0:T(4,128)}, u32[]{:S(2)}) copy-start(f32[3,1024]{1,0:T(4,128)} %param.12) | copy-start | bytes 36868
  151.7 5.8 %copy-start.3 = (f32[3,1024]{1,0:T(4,128)S(1)}, f32[3,1024]{1,0:T(4,128)}, u32[]{:S(2)}) copy-start(f32[3,1024]{1,0:T(4,128)} %param.13) | copy-start | bytes 36868
  151.7 26.9 %copy-start = (bf16[3,4,256,256]{3,2,1,0:T(8,128)(2,1)S(1)}, bf16[3,4,256,256]{3,2,1,0:T(8,128)(2,1)}, u32[]{:S(2)}) copy-start(bf16[3,4,256,256]{3,2,1,0:T(8,128)(2,1)} %param.9) | copy-start | bytes 4718596
  156.8 119.5 %all-gather.10.cloned.1.call-start = ((), (), s32[]{:S(2)}) async-start(), calls=%async_computation.6 | async-start | bytes 7077888 | tf_op jit(solution)/shard_map/all_gather | solution.py:38
  157.4 165.5 %reduce-scatter.6.cloned.1.call-start = ((), (), s32[]{:S(2)}) async-start(), calls=%async_computation.7 | async-start | bytes 1966080 | tf_op jit(solution)/shard_map/reduce_scatter | solution.py:44
  295.2 64.7 %all-gather.12.cloned.1.call-start = ((), (), s32[]{:S(2)}) async-start(), calls=%async_computation.8 | async-start | bytes 1966080 | tf_op jit(solution)/shard_map/all_gather | solution.py:72
  323.8 6.2 %collective-permute-start.2 = (bf16[256,8]{1,0:T(8,128)(2,1)S(1)}, bf16[256,8]{1,0:T(8,128)(2,1)S(1)}, u32[]{:S(2)}, u32[]{:S(2)}) collective-permute-start(bf16[256,8]{1,0:T(8,128)(2,1)S(1)} %get-tuple-element.22), channel_id=1, source_target_pairs={{0,4},{4,8},{8,12},{12,16},{16,20},{20,24},{24,28},{1,5},{5,9},{9,... | collective-permute-start | bytes 12296 | tf_op jit(solution)/shard_map/ppermute | solution.py:17
  326.9 5.0 %collective-permute-start.3 = (bf16[256,8]{1,0:T(8,128)(2,1)S(1)}, bf16[256,8]{1,0:T(8,128)(2,1)S(1)}, u32[]{:S(2)}, u32[]{:S(2)}) collective-permute-start(bf16[256,8]{1,0:T(8,128)(2,1)S(1)} %get-tuple-element.23), channel_id=1, source_target_pairs={{4,0},{8,4},{12,8},{16,12},{20,16},{24,20},{28,24},{5,1},{9,5},{13... | collective-permute-start | bytes 12296 | tf_op jit(solution)/shard_map/ppermute | solution.py:18
  338.2 70.6 %reduce-scatter.8.cloned.1.call-start = ((), (), s32[]{:S(2)}) async-start(), calls=%async_computation.9 | async-start | bytes 1966080 | tf_op jit(solution)/shard_map/reduce_scatter | solution.py:44
  359.9 2.4 copy-start.4
  379.4 66.4 %all-gather.14.cloned.1.call-start = ((), (), s32[]{:S(2)}) async-start(), calls=%async_computation.10 | async-start | bytes 1966080 | tf_op jit(solution)/shard_map/all_gather | solution.py:72
  409.7 6.2 %collective-permute-start.4 = (bf16[256,8]{1,0:T(8,128)(2,1)S(1)}, bf16[256,8]{1,0:T(8,128)(2,1)S(1)}, u32[]{:S(2)}, u32[]{:S(2)}) collective-permute-start(bf16[256,8]{1,0:T(8,128)(2,1)S(1)} %get-tuple-element.20), channel_id=1, source_target_pairs={{0,4},{4,8},{8,12},{12,16},{16,20},{20,24},{24,28},{1,5},{5,9},{9,... | collective-permute-start | bytes 12296 | tf_op jit(solution)/shard_map/ppermute | solution.py:17
  412.8 5.0 %collective-permute-start.5 = (bf16[256,8]{1,0:T(8,128)(2,1)S(1)}, bf16[256,8]{1,0:T(8,128)(2,1)S(1)}, u32[]{:S(2)}, u32[]{:S(2)}) collective-permute-start(bf16[256,8]{1,0:T(8,128)(2,1)S(1)} %get-tuple-element.21), channel_id=1, source_target_pairs={{4,0},{8,4},{12,8},{16,12},{20,16},{24,20},{28,24},{5,1},{9,5},{13... | collective-permute-start | bytes 12296 | tf_op jit(solution)/shard_map/ppermute | solution.py:18
  445.8 2.4 copy-start.5
Sparse Core Ops, SparseCore 0:
  9.4 98.0 all-gather.5
  112.7 28.6 reduce-scatter.3
  156.9 21.5 all-gather.7
  180.6 95.6 all-gather.9
  295.3 27.4 reduce-scatter.5
  338.3 21.5 all-gather.11
  379.6 29.1 reduce-scatter.7
  424.2 21.6 all-gather.13
where the time goes:
time: 469 us; the launch traced here: 466 us
  waiting for transfers between devices  353 us (75%)
  matrix products  39.2 us (8%)
  other arithmetic  20.4 us (4%)
  starting transfers between devices  19 us (4%)
  blocking collectives  17.9 us (4%)
  between operations  13.8 us (3%)
    all_gather x1, waiting for transfers between devices, on_device(): lax.all_gather(in_proj, 'sp', axis=2, tiled=True)  100 us
    all_gather x1, waiting for transfers between devices, on_device(): lax.all_gather(out_proj, 'sp', axis=1, tiled=True)  95.7 us
    reduce_scatter x3, waiting for transfers between devices, on_device(): lax.psum_scatter(lax.dot_general(in_block, stream, (((0,), (1,)), ((), ()...  85.6 us
    all_gather x3, waiting for transfers between devices, on_device(): all_differ = lax.all_gather(differ, 'tp', axis=0, tiled=True)  64.3 us
    psum x3, blocking collectives, on_device(): lax.psum((jnp.sum(resid, axis=1), jnp.sum(resid * resid, axis=1)), 'tp')  17.9 us
    dot_general x3, matrix products, on_device(): lax.dot_general(in_block, stream, (((0,), (1,)), ((), ())), preferred_ele...  16.8 us
    dot_general x3, matrix products, on_device(): lax.dot_general(mixed_all, out_block, (((0,), (0,)), ((), ())), preferred...  16 us
    convert_element_type x3, other arithmetic, on_device(): differ = (pooled - projected.astype(jnp.float32)).astype(jnp.bfloat16)  15 us
  transfers between devices with their start and end apart: 14, of which 11 were waited for; matrix products, arithmetic and copies ran while one was open for 0% of the time, Pallas kernels for 0%

commit v1 on v0

--- a/solution.py
+++ b/solution.py
@@ -1,7 +1,15 @@
+import functools
+
 import jax
 import jax.numpy as jnp
 from jax import lax
+from jax.experimental import pallas as pl
+from jax.experimental.pallas import tpu as pltpu
 from jax.sharding import PartitionSpec as P
+
+MESH = pl.DeviceIdType.MESH
+F32 = jnp.float32
+BF16 = jnp.bfloat16
 
 pool_windows = (2, 4, 8, 16)
 norm_eps = 1e-05
@@ -89,6 +97,399 @@
     return stream
 
 
+def mixer_kernel(
+    cfg,
+    tok,
+    win,
+    mixw,
+    gain,
+    wout,
+    ngain,
+    nbias,
+    out,
+    in_all,
+    out_all,
+    strm,
+    part_send,
+    part_recv,
+    px_send,
+    px_recv,
+    ext,
+    mix_all,
+    resid,
+    lanes,
+    stat_send,
+    stat_recv,
+    mean_col,
+    rstd_col,
+    wsend,
+    wrecv,
+    hsend,
+    hrecv,
+    asend,
+    arecv,
+):
+    n_sp, n_tp, ydim, halo = cfg
+    zdim = n_sp // ydim
+    layers = win.shape[0]
+    rows_dev, feat = tok.shape
+    rows = strm.shape[0]
+    pad = max(pool_windows) // 2
+    gw = mixw.shape[1]
+    cw = win.shape[2]
+    ow = wout.shape[1]
+    seq = rows_dev * n_sp
+    model = feat * n_tp
+    alpha = (2.0 * layers) ** 0.25
+    big = rows // 2
+    small = rows // 4
+    out_tile = rows_dev // 4
+    me_sp = lax.axis_index("sp")
+    me = lax.axis_index("tp")
+    z = me_sp // ydim
+    y = me_sp % ydim
+    ypeer = z * ydim + (ydim - 1 - y)
+    core = me % 2
+    xid = me // 2
+    sib = xid * 2 + (1 - core)
+    xo = (1 - xid) * 2 + core
+
+    barrier = pltpu.get_barrier_semaphore()
+    for d in range(1, n_sp):
+        pl.semaphore_signal(barrier, inc=1, device_id=((me_sp + d) % n_sp, me), device_id_type=MESH)
+    for d in range(1, n_tp):
+        pl.semaphore_signal(barrier, inc=1, device_id=(me_sp, (me + d) % n_tp), device_id_type=MESH)
+    pl.semaphore_wait(barrier, n_sp + n_tp - 2)
+
+    def remote(src, dst, ssem, rsem, dev):
+        return pltpu.make_async_remote_copy(
+            src_ref=src, dst_ref=dst, send_sem=ssem, recv_sem=rsem, device_id=dev, device_id_type=MESH
+        )
+
+    def halo_up():
+        return remote(
+            tok.at[pl.ds(rows_dev - halo, halo)], strm.at[pl.ds(0, halo)],
+            hsend.at[0], hrecv.at[0], ((me_sp + 1) % n_sp, me),
+        )
+
+    def halo_down():
+        return remote(
+            tok.at[pl.ds(0, halo)], strm.at[pl.ds(halo + rows_dev, halo)],
+            hsend.at[1], hrecv.at[1], ((me_sp + n_sp - 1) % n_sp, me),
+        )
+
+    @pl.when(me_sp < n_sp - 1)
+    def _():
+        halo_up().start()
+
+    @pl.when(me_sp > 0)
+    def _():
+        halo_down().start()
+
+    def shard(b, s):
+        l = b // 2
+        if b % 2 == 0:
+            return in_all.at[l, :, pl.ds(pl.multiple_of(s * cw, cw), cw)]
+        return out_all.at[l, pl.ds(pl.multiple_of(s * ow, ow), ow), :]
+
+    def own(b):
+        return win.at[b // 2] if b % 2 == 0 else wout.at[b // 2]
+
+    def wy(b):
+        return remote(own(b), shard(b, me_sp), wsend.at[b, 0], wrecv.at[b, me_sp], (ypeer, me))
+
+    def wz(b, d):
+        dev = ((z + d) % zdim) * ydim + y
+        return remote(own(b), shard(b, me_sp), wsend.at[b, d], wrecv.at[b, me_sp], (dev, me))
+
+    def wrelay(b, d):
+        s = ((z + d) % zdim) * ydim + y
+        return remote(shard(b, s), shard(b, s), wsend.at[b, zdim - 1 + d], wrecv.at[b, s], (ypeer, me))
+
+    def issue(b):
+        wy(b).start()
+        for d in range(1, zdim):
+            wz(b, d).start()
+
+    def relay(b):
+        for d in range(1, zdim):
+            copy = wrelay(b, d)
+            copy.wait_recv()
+            copy.start()
+
+    def finish(b):
+        for d in range(zdim):
+            s = ((z + d) % zdim) * ydim + (ydim - 1 - y)
+            remote(shard(b, s), shard(b, s), wsend.at[b, 0], wrecv.at[b, s], (ypeer, me)).wait_recv()
+
+    blocks = 2 * layers
+    issue(0)
+    issue(1)
+
+    for l in range(layers):
+        in_all[l, :, pl.ds(pl.multiple_of(me_sp * cw, cw), cw)] = win[l]
+        out_all[l, pl.ds(pl.multiple_of(me_sp * ow, ow), ow), :] = wout[l]
+    strm[pl.ds(halo, rows_dev), :] = tok[...]
+
+    @pl.when(me_sp == 0)
+    def _():
+        strm[pl.ds(0, halo), :] = jnp.zeros((halo, feat), BF16)
+
+    @pl.when(me_sp == n_sp - 1)
+    def _():
+        strm[pl.ds(halo + rows_dev, halo), :] = jnp.zeros((halo, feat), BF16)
+
+    ext[pl.ds(0, pad), :] = jnp.zeros((pad, gw), F32)
+    ext[pl.ds(pad + rows, pad), :] = jnp.zeros((pad, gw), F32)
+    lanes[...] = jnp.zeros(lanes.shape, F32)
+    stat_send[...] = jnp.zeros(stat_send.shape, F32)
+    sb = lanes.shape[1] // 128
+
+    @pl.when(me_sp > 0)
+    def _():
+        halo_up().wait_recv()
+
+    @pl.when(me_sp < n_sp - 1)
+    def _():
+        halo_down().wait_recv()
+
+    def loop(count, body):
+        lax.fori_loop(0, count, lambda i, c: (body(i), c)[1], 0)
+
+    for l in range(layers):
+        relay(2 * l)
+        if 2 * l + 2 < blocks:
+            issue(2 * l + 2)
+        finish(2 * l)
+
+        def in_dot(r, g):
+            return jnp.dot(
+                strm[r, :],
+                in_all[l, :, pl.ds(pl.multiple_of(g * gw, gw), gw)],
+                preferred_element_type=F32,
+            )
+
+        def body1(i):
+            r = pl.ds(pl.multiple_of(i * big, 16), big)
+            for q in range(2):
+                part_send[q, r, :] = in_dot(r, q * 2 + (1 - core)).astype(BF16)
+
+        loop(2, body1)
+        cpart = remote(part_send, part_recv, asend.at[0], arecv.at[0], (me_sp, sib))
+        cpart.start()
+
+        def body2(i):
+            r = pl.ds(pl.multiple_of(i * big, 16), big)
+            resid[r, pl.ds(0, gw)] = in_dot(r, xo)
+            resid[r, pl.ds(gw, gw)] = in_dot(r, me)
+
+        loop(2, body2)
+        cpart.wait_recv()
+
+        def body3(i):
+            r = pl.ds(pl.multiple_of(i * small, 16), small)
+            px_send[r, :] = (resid[r, pl.ds(0, gw)] + part_recv[1 - xid, r, :].astype(F32)).astype(BF16)
+
+        loop(4, body3)
+        cpx = remote(px_send, px_recv, asend.at[1], arecv.at[1], (me_sp, xo))
+        cpx.start()
+
+        def body4(i):
+            r = pl.ds(pl.multiple_of(i * small, 16), small)
+            resid[r, pl.ds(gw, gw)] = resid[r, pl.ds(gw, gw)] + part_recv[xid, r, :].astype(F32)
+
+        loop(4, body4)
+        cpx.wait_recv()
+
+        def body5(i):
+            r = pl.ds(pl.multiple_of(i * small, 16), small)
+            total = resid[r, pl.ds(gw, gw)] + px_recv[r, :].astype(F32)
+            proj = total.astype(BF16).astype(F32)
+            pos = lax.broadcasted_iota(jnp.int32, (small, gw), 0) + (me_sp * rows_dev - halo + i * small)
+            proj = jnp.where((pos >= 0) & (pos < seq), proj, 0.0)
+            ext[pl.ds(pl.multiple_of(pad + i * small, 8), small), :] = proj
+
+        loop(4, body5)
+
+        def body6(i):
+            n = small + 2 * pad
+            v = ext[pl.ds(pl.multiple_of(i * small, 8), n), :]
+            w = v + pltpu.roll(v, 1, 0)
+            window = w
+            half = 1
+            for g in range(1, len(pool_windows)):
+                w = pltpu.roll(w, half, 0) + pltpu.roll(w, n - half, 0)
+                window = jnp.where(me == g, w, window)
+                half *= 2
+            span = jnp.left_shift(1, me)
+            pos = lax.broadcasted_iota(jnp.int32, (small, gw), 0) + (me_sp * rows_dev - halo + i * small)
+            count = jnp.minimum(pos + span, seq) - jnp.maximum(pos - span, 0)
+            count = jnp.maximum(count, 1).astype(F32)
+            differ = (window[pad : pad + small] / count - v[pad : pad + small]).astype(BF16)
+            mixed = jnp.dot(differ, mixw[l], preferred_element_type=F32) * gain[l]
+            r = pl.ds(pl.multiple_of(i * small, 16), small)
+            mix_all[r, pl.ds(pl.multiple_of(me * gw, gw), gw)] = mixed.astype(BF16)
+
+        loop(4, body6)
+
+        def msl(g):
+            return mix_all.at[:, pl.ds(pl.multiple_of(g * gw, gw), gw)]
+
+        c_x = remote(msl(me), msl(me), asend.at[2], arecv.at[2], (me_sp, xo))
+        c_s = remote(msl(me), msl(me), asend.at[3], arecv.at[3], (me_sp, sib))
+        c_x.start()
+        c_s.start()
+        relay(2 * l + 1)
+        if 2 * l + 3 < blocks:
+            issue(2 * l + 3)
+        c_r = remote(msl(xo), msl(xo), asend.at[4], arecv.at[4], (me_sp, sib))
+        remote(msl(xo), msl(xo), asend.at[2], arecv.at[2], (me_sp, xo)).wait_recv()
+        c_r.start()
+        finish(2 * l + 1)
+        remote(msl(sib), msl(sib), asend.at[3], arecv.at[3], (me_sp, sib)).wait_recv()
+        dia = (1 - xid) * 2 + (1 - core)
+        remote(msl(dia), msl(dia), asend.at[4], arecv.at[4], (me_sp, sib)).wait_recv()
+
+        def body7(i):
+            r = pl.ds(pl.multiple_of(i * small, 16), small)
+            branch = jnp.dot(mix_all[r, :], out_all[l], preferred_element_type=F32)
+            res = alpha * strm[r, :].astype(F32) + branch
+            resid[r, :] = res
+            sq = res * res
+            a = res[:, 0:128]
+            b = sq[:, 0:128]
+            for k in range(1, feat // 128):
+                a = a + res[:, k * 128 : (k + 1) * 128]
+                b = b + sq[:, k * 128 : (k + 1) * 128]
+            lanes[0, r, :] = a
+            lanes[1, r, :] = b
+
+        loop(4, body7)
+        for k in range(sb):
+            for q in range(2):
+                blk = lanes[q, k * 128 : (k + 1) * 128, :]
+                stat_send[k : k + 1, q * 128 : (q + 1) * 128] = jnp.sum(blk.T, axis=0, keepdims=True)
+        stats = []
+        for d in range(1, n_tp):
+            c = remote(
+                stat_send, stat_recv.at[d - 1], asend.at[4 + d], arecv.at[4 + d], (me_sp, (me + d) % n_tp)
+            )
+            c.start()
+            stats.append(c)
+        for c in stats:
+            c.wait_recv()
+        total = stat_send[...]
+        for d in range(1, n_tp):
+            total = total + stat_recv[d - 1]
+        mean = total[:, 0:128] / model
+        var = total[:, 128:256] / model - mean * mean
+        rstd = lax.rsqrt(var + norm_eps)
+        for k in range(sb):
+            mean_col[k * 128 : (k + 1) * 128, :] = jnp.broadcast_to(mean[k : k + 1, :], (128, 128)).T
+            rstd_col[k * 128 : (k + 1) * 128, :] = jnp.broadcast_to(rstd[k : k + 1, :], (128, 128)).T
+
+        def normed(r, k):
+            ks = pl.ds(k * 128, 128)
+            t = (resid[r, ks] - mean_col[r, :]) * rstd_col[r, :]
+            return (t * ngain[l, :, ks] + nbias[l, :, ks]).astype(BF16)
+
+        last = l == layers - 1
+
+        def body8(i):
+            if last:
+                r = pl.ds(pl.multiple_of(halo + i * out_tile, 16), out_tile)
+                o = pl.ds(pl.multiple_of(i * out_tile, 16), out_tile)
+            else:
+                r = pl.ds(pl.multiple_of(i * small, 16), small)
+            for k in range(feat // 128):
+                if last:
+                    out[o, pl.ds(k * 128, 128)] = normed(r, k)
+                else:
+                    strm[r, pl.ds(k * 128, 128)] = normed(r, k)
+
+        loop(4, body8)
+        for c in [cpart, cpx, c_x, c_s, c_r] + stats:
+            c.wait_send()
+
+    @pl.when(me_sp < n_sp - 1)
+    def _():
+        halo_up().wait_send()
+
+    @pl.when(me_sp > 0)
+    def _():
+        halo_down().wait_send()
+
+    for b in range(blocks):
+        wy(b).wait_send()
+        for d in range(1, zdim):
+            wz(b, d).wait_send()
+            wrelay(b, d).wait_send()
+
+
+def in_one_kernel(n_sp, n_tp, tokens, in_proj, group_mix, pool_gain, out_proj, norm_gain, norm_bias):
+    rows_dev, feat = tokens.shape
+    layers = in_proj.shape[0]
+    gw = group_mix.shape[2]
+    width = in_proj.shape[2] * n_sp
+    ydim = 2
+    halo = -(-layers * (max(pool_windows) // 2) // 32) * 32
+    rows = rows_dev + 2 * halo
+    rows_pad = -(-rows // 128) * 128
+    me = lax.axis_index("tp")
+    mixw = lax.dynamic_index_in_dim(group_mix, me, axis=1, keepdims=False)
+    gain = lax.dynamic_slice_in_dim(pool_gain, me * gw, gw, axis=1)[:, None, :]
+    pad = max(pool_windows) // 2
+    vmem = pl.BlockSpec(memory_space=pltpu.VMEM)
+    zdim = n_sp // ydim
+    blocks = 2 * layers
+    return pl.pallas_call(
+        functools.partial(mixer_kernel, (n_sp, n_tp, ydim, halo)),
+        out_shape=jax.ShapeDtypeStruct((rows_dev, feat), BF16),
+        in_specs=[vmem] * 7,
+        out_specs=vmem,
+        scratch_shapes=[
+            pltpu.VMEM((layers, feat, width), BF16),
+            pltpu.VMEM((layers, width, feat), BF16),
+            pltpu.VMEM((rows, feat), BF16),
+            pltpu.VMEM((2, rows, gw), BF16),
+            pltpu.VMEM((2, rows, gw), BF16),
+            pltpu.VMEM((rows, gw), BF16),
+            pltpu.VMEM((rows, gw), BF16),
+            pltpu.VMEM((rows + 2 * pad, gw), F32),
+            pltpu.VMEM((rows, width), BF16),
+            pltpu.VMEM((rows, feat), F32),
+            pltpu.VMEM((2, rows_pad, 128), F32),
+            pltpu.VMEM((-(-rows_pad // 1024) * 8, 256), F32),
+            pltpu.VMEM((n_tp - 1, -(-rows_pad // 1024) * 8, 256), F32),
+            pltpu.VMEM((rows_pad, 128), F32),
+            pltpu.VMEM((rows_pad, 128), F32),
+            pltpu.SemaphoreType.DMA((blocks, 2 * zdim - 1)),
+            pltpu.SemaphoreType.DMA((blocks, n_sp)),
+            pltpu.SemaphoreType.DMA((2,)),
+            pltpu.SemaphoreType.DMA((2,)),
+            pltpu.SemaphoreType.DMA((4 + n_tp,)),
+            pltpu.SemaphoreType.DMA((4 + n_tp,)),
+        ],
+        compiler_params=pltpu.CompilerParams(
+            collective_id=0, has_side_effects=True, vmem_limit_bytes=60 * 1024 * 1024
+        ),
+    )(tokens, in_proj, mixw, gain, out_proj, norm_gain[:, None, :], norm_bias[:, None, :])
+
+
+def one_kernel_fits(n_sp, n_tp, tokens, in_proj, group_mix):
+    rows_dev = tokens.shape[0] // n_sp
+    return (
+        n_tp == 4
+        and group_mix.shape[1] == n_tp
+        and in_proj.shape[2] == n_tp * group_mix.shape[2]
+        and group_mix.shape[2] % 128 == 0
+        and n_sp % 2 == 0
+        and (in_proj.shape[2] // n_sp) % 128 == 0
+        and rows_dev % 64 == 0
+        and (tokens.shape[1] // n_tp) % 128 == 0
+    )
+
+
 def solution(mesh):
     in_specs = (
         P("sp", "tp"),
@@ -100,6 +501,14 @@
         P(None, "tp"),
     )
     out_specs = P("sp", "tp")
-    return jax.shard_map(
-        on_device, mesh=mesh, in_specs=in_specs, out_specs=out_specs, check_vma=False
-    )
+    n_sp, n_tp = mesh.shape["sp"], mesh.shape["tp"]
+
+    def run(tokens, in_proj, group_mix, *rest):
+        body = on_device
+        if one_kernel_fits(n_sp, n_tp, tokens, in_proj, group_mix):
+            body = functools.partial(in_one_kernel, n_sp, n_tp)
+        return jax.shard_map(
+            body, mesh=mesh, in_specs=in_specs, out_specs=out_specs, check_vma=False
+        )(tokens, in_proj, group_mix, *rest)
+
+    return run

time: 469 us -> 236 us (0.50)
  waiting for transfers between devices: 353 us -> 0 us
  Pallas kernels: 0 us -> 228 us
  matrix products: 39.2 us -> 0 us
  other arithmetic: 20.4 us -> 0 us
  starting transfers between devices: 19 us -> 0 us
  blocking collectives: 17.9 us -> 0 us
  between operations: 13.8 us -> 0.01 us
    all_gather x5 -> x0, waiting for transfers between devices: 260 us -> none  [the longest x1 100 us: on_device(): lax.all_gather(in_proj, 'sp', axis=2, tiled=True)]
    pallas_call x0 -> x1, Pallas kernels: none -> 228 us  [in_one_kernel(): pl.pallas_call(functools.partial(mixer_kernel, (n_sp, n_tp, ydim, halo)),...]
    reduce_scatter x3 -> x0, waiting for transfers between devices: 85.6 us -> none  [on_device(): lax.psum_scatter(lax.dot_general(in_block, stream, (((0,), (1,)), ((), ()...]
    dot_general x9 -> x0, matrix products: 39.2 us -> none  [the longest x3 16.8 us: on_device(): lax.dot_general(in_block, stream, (((0,), (1,)), ((), ())), preferred_ele...]
    convert_element_type x9 -> x0, other arithmetic: 20.3 us -> none  [the longest x3 15 us: on_device(): differ = (pooled - projected.astype(jnp.float32)).astype(jnp.bfloat16)]
    ppermute x6 -> x0, starting transfers between devices: 18.5 us -> none  [the longest x3 9.31 us: padded(): before = lax.ppermute(last, axis, up)]
    psum x3 -> x0, blocking collectives: 17.9 us -> none  [on_device(): lax.psum((jnp.sum(resid, axis=1), jnp.sum(resid * resid, axis=1)), 'tp')]
    ppermute x6 -> x0, waiting for transfers between devices: 5.73 us -> none  [the longest x3 5.72 us: padded(): after = lax.ppermute(leading, axis, down)]
  transfers between devices with their start and end apart: 14 -> 0, of which waited for: 11 -> 0; matrix products, arithmetic and copies ran while one was open for 0% -> 0% of each run, Pallas kernels for 0% -> 0%
where the time goes in v1:
time: 236 us
  Pallas kernels  228 us (97%)
  local copies, waits for them, and re-layouts  7.49 us (3%)
    pallas_call x1, Pallas kernels, in_one_kernel(): pl.pallas_call(functools.partial(mixer_kernel, (n_sp, n_tp, ydim, halo)),...  228 us

profile of v1, /device:TPU:9, one launch (start us, length us, event | category | flops | bytes accessed | tf_op | source)
XLA Modules:
  0.0 235.7 jit_solution(9793303904356311898)
XLA Ops:
  0.0 0.0 copy-start
  0.0 0.8 constant_dynamic-slice_fusion
  0.8 0.6 broadcast_in_dim.9.gain
  1.4 1.3 broadcast_in_dim.10.ngain
  2.7 1.3 broadcast_in_dim.11.nbias
  4.0 0.0 copy-done
  4.1 0.8 dynamic-slice_bitcast_fusion.mixw
  4.8 228.2 %shard_map.73 = bf16[768,1024]{1,0:T(8,128)(2,1)} custom-call(bf16[768,1024]{1,0:T(8,128)(2,1)} %tok.1, bf16[3,1024,128]{2,1,0:T(8,128)(2,1)} %win.1, bf16[3,256,256]{2,1,0:T(8,128)(2,1)} %dynamic-slice_bitcast_fusion.mixw, f32[3,1,256]{2,1,0:T(1,128)} %broadcast_in_dim.9.gain, bf16[3,128,1024]{2,1,0:T(8,128)(2,1)} %wout.1, ...), custom_call_target="tpu_custom_call" | custom-call | tf_op jit(solution)/shard_map/pallas_call | solution.py:445
  233.0 2.7 %copy.9 = bf16[768,1024]{1,0:T(8,128)(2,1)} copy(bf16[768,1024]{1,0:T(8,128)(2,1)} %shard_map.73) | data formatting | bytes 3145728
Async XLA Ops:
  0.0 4.0 %copy-start = (bf16[3,4,256,256]{3,2,1,0:T(8,128)(2,1)S(1)}, bf16[3,4,256,256]{3,2,1,0:T(8,128)(2,1)}, u32[]{:S(2)}) copy-start(bf16[3,4,256,256]{3,2,1,0:T(8,128)(2,1)} %param.9) | copy-start | bytes 4718596

commit v2 on v1

--- a/solution.py
+++ b/solution.py
@@ -195,36 +195,99 @@
     def own(b):
         return win.at[b // 2] if b % 2 == 0 else wout.at[b // 2]
 
-    def wy(b):
-        return remote(own(b), shard(b, me_sp), wsend.at[b, 0], wrecv.at[b, me_sp], (ypeer, me))
-
-    def wz(b, d):
-        dev = ((z + d) % zdim) * ydim + y
-        return remote(own(b), shard(b, me_sp), wsend.at[b, d], wrecv.at[b, me_sp], (dev, me))
-
-    def wrelay(b, d):
-        s = ((z + d) % zdim) * ydim + y
-        return remote(shard(b, s), shard(b, s), wsend.at[b, zdim - 1 + d], wrecv.at[b, s], (ypeer, me))
+    yf_block = -1
+    blocks = 2 * layers
+    top = z < zdim - 1
+    low = z > 0
+
+    def fwd(b, s, src, kind):
+        dev = (ypeer, (me_sp + ydim) % n_sp, (me_sp + n_sp - ydim) % n_sp)[kind]
+        return remote(src, shard(b, s), wsend.at[b, kind, s], wrecv.at[b, s], (dev, me))
+
+    def arrived(b, s):
+        fwd(b, s, shard(b, s), 0).wait_recv()
+
+    def send(b, s, src, kind, cond=None):
+        if cond is None:
+            fwd(b, s, src, kind).start()
+        else:
+
+            @pl.when(cond)
+            def _():
+                fwd(b, s, src, kind).start()
 
     def issue(b):
-        wy(b).start()
-        for d in range(1, zdim):
-            wz(b, d).start()
-
-    def relay(b):
-        for d in range(1, zdim):
-            copy = wrelay(b, d)
-            copy.wait_recv()
-            copy.start()
+        send(b, me_sp, own(b), 1, top)
+        send(b, me_sp, own(b), 2, low)
+        send(b, me_sp, own(b), 0)
+
+    def step(b, k):
+        if k == 0:
+            s0 = ypeer
+            arrived(b, s0)
+            send(b, s0, shard(b, s0), 1, top)
+            send(b, s0, shard(b, s0), 2, low)
+            return
+        yf = b == yf_block
+        for base in (me_sp, ypeer) if yf else (me_sp,):
+
+            @pl.when(z >= k)
+            def _():
+                sb = base - k * ydim
+                arrived(b, sb)
+                send(b, sb, shard(b, sb), 1, top)
+                if not yf:
+                    send(b, sb, shard(b, sb), 0)
+
+            @pl.when(z + k < zdim)
+            def _():
+                sa = base + k * ydim
+                arrived(b, sa)
+                send(b, sa, shard(b, sa), 2, low)
+                if not yf:
+                    send(b, sa, shard(b, sa), 0)
 
     def finish(b):
-        for d in range(zdim):
-            s = ((z + d) % zdim) * ydim + (ydim - 1 - y)
-            remote(shard(b, s), shard(b, s), wsend.at[b, 0], wrecv.at[b, s], (ypeer, me)).wait_recv()
-
-    blocks = 2 * layers
-    issue(0)
-    issue(1)
+        if b != yf_block:
+            for d in range(zdim):
+                arrived(b, ((z + d) % zdim) * ydim + (ydim - 1 - y))
+
+    def drain(b):
+        yf = b == yf_block
+        fwd(b, me_sp, own(b), 0).wait_send()
+        for k in range(zdim):
+            if k > 0 and not yf:
+                s = ((z + k) % zdim) * ydim + y
+                fwd(b, s, shard(b, s), 0).wait_send()
+            for base in (me_sp, ypeer) if yf else (me_sp,):
+
+                @pl.when((z >= k) & top)
+                def _():
+                    sb = base - k * ydim
+                    fwd(b, sb, shard(b, sb), 1).wait_send()
+
+                @pl.when((z + k < zdim) & low)
+                def _():
+                    sa = base + k * ydim
+                    fwd(b, sa, shard(b, sa), 2).wait_send()
+
+    events = [(b, k) for b in range(blocks) for k in range(0 if b == yf_block else 1, zdim)]
+    ahead = 3
+
+    def pump(count):
+        for _ in range(min(count, len(events))):
+            b, k = events.pop(0)
+            step(b, k)
+            if k == zdim - 1 and b + ahead < blocks:
+                issue(b + ahead)
+
+    def need(b):
+        while events and events[0][0] <= b:
+            pump(1)
+        finish(b)
+
+    for b in range(min(ahead, blocks)):
+        issue(b)
 
     for l in range(layers):
         in_all[l, :, pl.ds(pl.multiple_of(me_sp * cw, cw), cw)] = win[l]
@@ -257,10 +320,7 @@
         lax.fori_loop(0, count, lambda i, c: (body(i), c)[1], 0)
 
     for l in range(layers):
-        relay(2 * l)
-        if 2 * l + 2 < blocks:
-            issue(2 * l + 2)
-        finish(2 * l)
+        need(2 * l)
 
         def in_dot(r, g):
             return jnp.dot(
@@ -277,6 +337,7 @@
         loop(2, body1)
         cpart = remote(part_send, part_recv, asend.at[0], arecv.at[0], (me_sp, sib))
         cpart.start()
+        pump(1)
 
         def body2(i):
             r = pl.ds(pl.multiple_of(i * big, 16), big)
@@ -293,12 +354,14 @@
         loop(4, body3)
         cpx = remote(px_send, px_recv, asend.at[1], arecv.at[1], (me_sp, xo))
         cpx.start()
+        pump(2)
 
         def body4(i):
             r = pl.ds(pl.multiple_of(i * small, 16), small)
             resid[r, pl.ds(gw, gw)] = resid[r, pl.ds(gw, gw)] + part_recv[xid, r, :].astype(F32)
 
         loop(4, body4)
+        pump(2)
         cpx.wait_recv()
 
         def body5(i):
@@ -332,6 +395,8 @@
 
         loop(4, body6)
 
+        pump(1)
+
         def msl(g):
             return mix_all.at[:, pl.ds(pl.multiple_of(g * gw, gw), gw)]
 
@@ -339,13 +404,11 @@
         c_s = remote(msl(me), msl(me), asend.at[3], arecv.at[3], (me_sp, sib))
         c_x.start()
         c_s.start()
-        relay(2 * l + 1)
-        if 2 * l + 3 < blocks:
-            issue(2 * l + 3)
+        pump(1)
         c_r = remote(msl(xo), msl(xo), asend.at[4], arecv.at[4], (me_sp, sib))
         remote(msl(xo), msl(xo), asend.at[2], arecv.at[2], (me_sp, xo)).wait_recv()
         c_r.start()
-        finish(2 * l + 1)
+        need(2 * l + 1)
         remote(msl(sib), msl(sib), asend.at[3], arecv.at[3], (me_sp, sib)).wait_recv()
         dia = (1 - xid) * 2 + (1 - core)
         remote(msl(dia), msl(dia), asend.at[4], arecv.at[4], (me_sp, sib)).wait_recv()
@@ -376,6 +439,7 @@
             )
             c.start()
             stats.append(c)
+        pump(2)
         for c in stats:
             c.wait_recv()
         total = stat_send[...]
@@ -420,10 +484,7 @@
         halo_down().wait_send()
 
     for b in range(blocks):
-        wy(b).wait_send()
-        for d in range(1, zdim):
-            wz(b, d).wait_send()
-            wrelay(b, d).wait_send()
+        drain(b)
 
 
 def in_one_kernel(n_sp, n_tp, tokens, in_proj, group_mix, pool_gain, out_proj, norm_gain, norm_bias):
@@ -463,7 +524,7 @@
             pltpu.VMEM((n_tp - 1, -(-rows_pad // 1024) * 8, 256), F32),
             pltpu.VMEM((rows_pad, 128), F32),
             pltpu.VMEM((rows_pad, 128), F32),
-            pltpu.SemaphoreType.DMA((blocks, 2 * zdim - 1)),
+            pltpu.SemaphoreType.DMA((blocks, 3, n_sp)),
             pltpu.SemaphoreType.DMA((blocks, n_sp)),
             pltpu.SemaphoreType.DMA((2,)),
             pltpu.SemaphoreType.DMA((2,)),

time: 236 us -> 178 us (0.75); the launches traced: 236 us -> 174 us
  Pallas kernels: 228 us -> 167 us
    pallas_call x1, Pallas kernels: 228 us -> 167 us  [in_one_kernel(): pl.pallas_call(functools.partial(mixer_kernel, (n_sp, n_tp, ydim, halo)),...]
where the time goes in v2:
time: 178 us; the launch traced here: 174 us
  Pallas kernels  167 us (94%)
  local copies, waits for them, and re-layouts  7.49 us (4%)
    pallas_call x1, Pallas kernels, in_one_kernel(): pl.pallas_call(functools.partial(mixer_kernel, (n_sp, n_tp, ydim, halo)),...  167 us

profile of v2, /device:TPU:9, one launch (start us, length us, event | category | flops | bytes accessed | tf_op | source)
XLA Modules:
  0.0 174.5 jit_solution(16380604886906309781)
XLA Ops:
  0.0 0.0 copy-start
  0.0 0.8 constant_dynamic-slice_fusion
  0.8 0.6 broadcast_in_dim.9.gain
  1.4 1.3 broadcast_in_dim.10.ngain
  2.7 1.3 broadcast_in_dim.11.nbias
  4.0 0.0 copy-done
  4.1 0.8 dynamic-slice_bitcast_fusion.mixw
  4.8 167.0 %shard_map.73 = bf16[768,1024]{1,0:T(8,128)(2,1)} custom-call(bf16[768,1024]{1,0:T(8,128)(2,1)} %tok.1, bf16[3,1024,128]{2,1,0:T(8,128)(2,1)} %win.1, bf16[3,256,256]{2,1,0:T(8,128)(2,1)} %dynamic-slice_bitcast_fusion.mixw, f32[3,1,256]{2,1,0:T(1,128)} %broadcast_in_dim.9.gain, bf16[3,128,1024]{2,1,0:T(8,128)(2,1)} %wout.1, ...), custom_call_target="tpu_custom_call" | custom-call | tf_op jit(solution)/shard_map/pallas_call | solution.py:506
  171.8 2.7 %copy.9 = bf16[768,1024]{1,0:T(8,128)(2,1)} copy(bf16[768,1024]{1,0:T(8,128)(2,1)} %shard_map.73) | data formatting | bytes 3145728
Async XLA Ops:
  0.0 4.0 %copy-start = (bf16[3,4,256,256]{3,2,1,0:T(8,128)(2,1)S(1)}, bf16[3,4,256,256]{3,2,1,0:T(8,128)(2,1)}, u32[]{:S(2)}) copy-start(bf16[3,4,256,256]{3,2,1,0:T(8,128)(2,1)} %param.9) | copy-start | bytes 4718596
